TPU v7x, 1024 devices: a 2x16x16 block of a 4x16x16 slice. The times are simulated.
1024 devices in a mesh: grp: 2 (over x), fs: 16 (over z), tp: 32 (over y, core).
Axes of the slice: x: 2, y: 16, z: 16, core: 2. Of those that a mesh axis runs over, the one named last changes fastest.
The devices are a block of a 4x16x16 slice.
Arguments:
- tokens: bfloat16 [8192, 2048], P(('grp', 'fs')), parts along dimension 0, may hold values from -6 to 6
- routes: int32 [8192, 2], P(('grp', 'fs')), parts along dimension 0, may hold values from 0 to 15, all different within a row; in each aligned block of 256 rows (0 to 255, 256 to 511, ...) at most 48 rows name the same one
- route_logits: float32 [8192, 2], P(('grp', 'fs')), parts along dimension 0, may hold values from -6 to 6
- gain: float32 [2048], P('fs'), may hold values from 0.1 to 1.9
- w_gate: float32 [16, 2048, 4096], P(None, 'fs', 'tp'), may hold values from -0.125 to 0.125
- w_up: float32 [16, 2048, 4096], P(None, 'fs', 'tp'), may hold values from -0.125 to 0.125
- w_down: float32 [16, 2048, 4096], P(None, 'fs', 'tp'), may hold values from -0.09375 to 0.09375
Outputs:
- gate_out: bfloat16 [32, 2048, 4096], P(('grp', 'fs'), None, 'tp'), parts along dimension 0
- up_out: bfloat16 [32, 2048, 4096], P(('grp', 'fs'), None, 'tp'), parts along dimension 0
- down_out: bfloat16 [32, 2048, 4096], P(('grp', 'fs'), None, 'tp'), parts along dimension 0
- mixed: bfloat16 [8192, 2048], P(('grp', 'fs'), 'tp'), parts along dimension 0
There are 2 independent parts, one for each index of `grp`. A program takes and returns all parts, laid end to end along the dimension named above; an argument that names none is the same for every part. Nothing has to cross between parts.
Inputs may be any that keep to these rules, and one draw needn't show every extreme that they name: `routes`: each row names two different experts. In each aligned block of 256 rows (the tokens of one index of fs) no expert is named by more than 48 rows, a bound that some block reaches.
All inputs are finite; a program needn't handle non-finite values.
Results may differ from a plain program's by a relative error of at most 0.025.
Values may be sent and summed in bfloat16 or wider, within the bound.
A program may use at most 32 MiB of HBM per device.

v0:
```python
import jax
import jax.numpy as jnp
from jax import lax
from jax.sharding import Mesh
from jax.sharding import PartitionSpec as P

TP = ("tp_0", "tp_1")


EPS = 1e-06


def side_by_side(arrays, axis, split_dim, concat_dim, along):
    ends, at = ([], 0)
    for a in arrays[:-1]:
        at += a.shape[along]
        ends.append(at)
    both = jnp.concatenate(arrays, axis=along)
    return tuple(
        jnp.split(
            lax.all_to_all(both, axis, split_axis=split_dim, concat_axis=concat_dim, tiled=True),
            ends,
            axis=along,
        )
    )


def own_block(tiles, axes, sequence):
    inside = tiles.shape[1:]
    tiles = tiles.reshape(*(lax.axis_size(a) for a in axes), *inside)
    tiles = jnp.moveaxis(tiles, sequence, range(len(axes))).reshape(-1, *inside)
    for k in sequence:
        tiles = lax.psum_scatter(tiles, axes[k], scatter_dimension=0, tiled=True)
    return tiles[0]


def cut_along(value, dim, count):
    before, after = (value.shape[:dim], value.shape[dim + 1 :])
    return jnp.moveaxis(value.reshape(*before, count, -1, *after), dim, 0)


def sum_by_axis(value, axes, sequence, dim):
    count = lax.axis_size(axes)
    return own_block(cut_along(value, dim, count), axes, sequence)


def normalize(tokens):
    values = tokens.astype(jnp.float32)
    centred = values - jnp.mean(values, axis=-1, keepdims=True)
    spread = jnp.mean(centred * centred, axis=-1, keepdims=True)
    return (centred * lax.rsqrt(spread + EPS)).astype(jnp.bfloat16)


def on_device(tokens, routes, route_logits, gain, w_gate, w_up, w_down):
    folded_gate = (gain[None, :, None] * w_gate).astype(jnp.bfloat16)
    folded_up = (gain[None, :, None] * w_up).astype(jnp.bfloat16)
    rounded_down = w_down.astype(jnp.bfloat16)
    gate_out, up_out = side_by_side((folded_gate, folded_up), "fs", 0, 1, 2)
    down_out = lax.all_to_all(rounded_down, "fs", split_axis=0, concat_axis=1, tiled=True)
    experts = w_gate.shape[0]
    tok_rows = tokens.shape[0]
    capacity = 3 * tok_rows // experts
    normed = normalize(tokens)
    expert_ids = jnp.arange(experts, dtype=jnp.int32)
    chosen = routes[:, :, None] == expert_ids[None, None, :]
    marked = jnp.sum(chosen.astype(jnp.int32), axis=1)
    before = jnp.cumsum(marked, axis=0) - marked
    slot_ids = jnp.where(marked > 0, expert_ids[None, :] * capacity + before, -1)
    places = jnp.arange(experts * capacity, dtype=jnp.int32)
    matches = places[:, None, None] == slot_ids[None, :, :]
    picker = jnp.any(matches, axis=2).astype(jnp.bfloat16)
    diff = route_logits[:, 0] - route_logits[:, 1]
    shares = jax.nn.sigmoid(jnp.stack([diff, -diff], axis=1))
    weight_table = jnp.sum(chosen.astype(jnp.float32) * shares[:, :, None], axis=1)
    combine = jnp.sum(
        jnp.where(jnp.transpose(matches, (1, 2, 0)), weight_table[:, :, None], 0.0), axis=1
    )
    gate_local = gate_out[0]
    up_local = up_out[0]
    outbound = jnp.dot(picker, normed, preferred_element_type=jnp.float32).astype(jnp.bfloat16)
    arrived = lax.all_to_all(outbound, "fs", split_axis=0, concat_axis=0, tiled=True)
    gate_sum = jnp.dot(arrived, gate_local, preferred_element_type=jnp.float32)
    up_sum = jnp.dot(arrived, up_local, preferred_element_type=jnp.float32)
    hidden = (jax.nn.silu(gate_sum) * up_sum).astype(jnp.bfloat16)
    down_local = down_out[0]
    summed = sum_by_axis(
        lax.dot_general(
            down_local, hidden, (((1,), (1,)), ((), ())), preferred_element_type=jnp.float32
        ).astype(jnp.bfloat16),
        TP,
        (1, 0),
        0,
    ).astype(jnp.float32)
    results = summed.astype(jnp.bfloat16)
    returned = lax.all_to_all(results, "fs", split_axis=1, concat_axis=1, tiled=True)
    mixed_out = lax.dot_general(
        combine,
        returned.astype(jnp.float32),
        (((1,), (1,)), ((), ())),
        precision=lax.Precision.HIGHEST,
        preferred_element_type=jnp.float32,
    )
    return (gate_out, up_out, down_out, mixed_out.astype(jnp.bfloat16))


def solution(mesh):
    finer = Mesh(
        mesh.devices.reshape(mesh.shape["grp"], mesh.shape["fs"], 16, 2),
        ("grp", "fs", "tp_0", "tp_1"),
    )
    in_specs = (
        P(("grp", "fs"), None),
        P(("grp", "fs"), None),
        P(("grp", "fs"), None),
        P("fs"),
        P(None, "fs", TP),
        P(None, "fs", TP),
        P(None, "fs", TP),
    )
    out_specs = (
        P(("grp", "fs"), None, TP),
        P(("grp", "fs"), None, TP),
        P(("grp", "fs"), None, TP),
        P(("grp", "fs"), TP),
    )
    return jax.shard_map(
        on_device, mesh=finer, in_specs=in_specs, out_specs=out_specs, check_vma=False
    )
```

profile of v0, /device:TPU:6, one launch (start us, length us, event | category | flops | bytes accessed | tf_op | source)
XLA Modules:
  0.0 488.6 jit_solution(11913942987818286068)
XLA Ops:
  7.2 2.0 multiply_convert_fusion.1
  9.2 1.1 pad_maximum_fusion
  10.3 83.1 %all-to-all-start = ((bf16[16,128,256]{2,1,0:T(8,128)(2,1)}), bf16[16,128,256]{2,1,0:T(8,128)(2,1)S(1)}, u32[]{:S(2)}, u32[]{:S(2)}) async-start(bf16[16,128,256]{2,1,0:T(8,128)(2,1)} %pad_maximum_fusion), calls=%async_computation | async-start | bytes 2097152 | tf_op jit(solution)/shard_map/all_to_all | solution.py:21
  95.0 3.1 fusion
  98.2 2.8 convolution_convert_fusion.1
  101.0 42.2 %all-to-all-done = bf16[16,128,256]{2,1,0:T(8,128)(2,1)S(1)} async-done(((bf16[16,128,256]{2,1,0:T(8,128)(2,1)}), bf16[16,128,256]{2,1,0:T(8,128)(2,1)S(1)}, u32[]{:S(2)}, u32[]{:S(2)}) %all-to-all-start) | async-done | bytes 1048608 | tf_op jit(solution)/shard_map/all_to_all | solution.py:21
  143.2 1.0 copy-done.1
  144.2 8.1 %all-to-all-start.2 = ((bf16[16,48,2048]{2,1,0:T(8,128)(2,1)}), bf16[16,48,2048]{2,1,0:T(8,128)(2,1)S(1)}, u32[]{:S(2)}, u32[]{:S(2)}) async-start(bf16[16,48,2048]{2,1,0:T(8,128)(2,1)} %bitcast.57), calls=%async_computation.2 | async-start | bytes 6291456 | tf_op jit(solution)/shard_map/all_to_all | solution.py:81
  152.3 2.1 convert_element_type.40
  154.5 136.9 %all-to-all-done.2 = bf16[16,48,2048]{2,1,0:T(8,128)(2,1)S(1)} async-done(((bf16[16,48,2048]{2,1,0:T(8,128)(2,1)}), bf16[16,48,2048]{2,1,0:T(8,128)(2,1)S(1)}, u32[]{:S(2)}, u32[]{:S(2)}) %all-to-all-start.2) | async-done | bytes 3145760 | tf_op jit(solution)/shard_map/all_to_all | solution.py:81
  291.4 8.9 %all-to-all-start.1 = ((bf16[16,128,128]{2,1,0:T(8,128)(2,1)}), bf16[16,128,128]{2,1,0:T(8,128)(2,1)}, u32[]{:S(2)}, u32[]{:S(2)}) async-start(bf16[16,128,128]{2,1,0:T(8,128)(2,1)} %convert_element_type.40), calls=%async_computation.1 | async-start | bytes 1048576 | tf_op jit(solution)/shard_map/all_to_all | solution.py:59
  300.4 2.1 fusion.28
  304.2 25.1 %all-to-all-done.1 = bf16[16,128,128]{2,1,0:T(8,128)(2,1)} async-done(((bf16[16,128,128]{2,1,0:T(8,128)(2,1)}), bf16[16,128,128]{2,1,0:T(8,128)(2,1)}, u32[]{:S(2)}, u32[]{:S(2)}) %all-to-all-start.1) | async-done | bytes 524320 | tf_op jit(solution)/shard_map/all_to_all | solution.py:59
  329.4 6.2 %fusion.1 = bf16[2048,768]{0,1:T(8,128)(2,1)} fusion(bf16[2048,128]{1,0:T(8,128)(2,1)} %bitcast.8, bf16[768,2048]{1,0:T(8,128)(2,1)S(1)} %bitcast.54, bf16[1,2048,128]{2,1,0:T(8,128)(2,1)} %get-tuple-element.15, f32[768,128]{1,0:T(8,128)S(1)} %fusion.12), kind=kOutput, calls=%fused_computation.6 | convolution fusion | flops 807469056 | bytes 7733248 | tf_op jit(solution)/shard_map/dot_general | solution.py:87
  335.6 3.2 copy.35
  338.7 1.9 copy.36
  340.8 25.6 %reduce-scatter.3.cloned.1.call-done = bf16[16,64,768]{2,1,0:T(8,128)(2,1)} async-done(((bf16[32,64,768]{2,1,0:T(8,128)(2,1)}), bf16[16,64,768]{2,1,0:T(8,128)(2,1)}) %reduce-scatter.3.cloned.1.call-update) | async-done | bytes 1572880 | tf_op jit(solution)/shard_map/reduce_scatter | solution.py:33
  366.7 83.4 %reduce-scatter.5.cloned.1.call-done = bf16[1,64,768]{2,1,0:T(8,128)(2,1)} async-done(((bf16[16,64,768]{2,1,0:T(8,128)(2,1)}), bf16[1,64,768]{2,1,0:T(8,128)(2,1)}) %reduce-scatter.5.cloned.1.call-update) | async-done | bytes 98320 | tf_op jit(solution)/shard_map/reduce_scatter | solution.py:33
  450.1 1.1 copy.39
  451.9 13.8 %all-to-all-start.3 = ((bf16[16,2,1536]{2,1,0:T(2,128)(2,1)}), bf16[16,2,1536]{2,1,0:T(2,128)(2,1)S(1)}, u32[]{:S(2)}, u32[]{:S(2)}) async-start(bf16[16,2,1536]{2,1,0:T(2,128)(2,1)} %reshape.76), calls=%async_computation.5 | async-start | bytes 196608 | tf_op jit(solution)/shard_map/all_to_all | solution.py:95
  465.7 3.0 select_reduce_fusion
  468.7 9.8 %all-to-all-done.3 = bf16[16,2,1536]{2,1,0:T(2,128)(2,1)S(1)} async-done(((bf16[16,2,1536]{2,1,0:T(2,128)(2,1)}), bf16[16,2,1536]{2,1,0:T(2,128)(2,1)S(1)}, u32[]{:S(2)}, u32[]{:S(2)}) %all-to-all-start.3) | async-done | bytes 98336 | tf_op jit(solution)/shard_map/all_to_all | solution.py:95
  478.7 1.1 convolution_convert_fusion.2
  479.8 1.9 copy.46
  (35 shorter events, 4.8 us)
Async XLA Ops:
  7.2 86.2 %copy-start.3 = (s32[256,2]{0,1:T(2,128)S(1)}, s32[256,2]{0,1:T(2,128)}, u32[]{:S(2)}) copy-start(s32[256,2]{0,1:T(2,128)} %param.8) | copy-start | bytes 6148
  7.2 87.1 %copy-start = (bf16[256,2048]{1,0:T(8,128)(2,1)S(1)}, bf16[256,2048]{1,0:T(8,128)(2,1)}, u32[]{:S(2)}) copy-start(bf16[256,2048]{1,0:T(8,128)(2,1)} %param.7) | copy-start | bytes 3145732
  10.3 132.9 %all-to-all-start = ((bf16[16,128,256]{2,1,0:T(8,128)(2,1)}), bf16[16,128,256]{2,1,0:T(8,128)(2,1)S(1)}, u32[]{:S(2)}, u32[]{:S(2)}) async-start(bf16[16,128,256]{2,1,0:T(8,128)(2,1)} %pad_maximum_fusion), calls=%async_computation | async-start | bytes 2097152 | tf_op jit(solution)/shard_map/all_to_all | solution.py:21
  143.2 1.0 copy-start.1
  144.2 147.2 %all-to-all-start.2 = ((bf16[16,48,2048]{2,1,0:T(8,128)(2,1)}), bf16[16,48,2048]{2,1,0:T(8,128)(2,1)S(1)}, u32[]{:S(2)}, u32[]{:S(2)}) async-start(bf16[16,48,2048]{2,1,0:T(8,128)(2,1)} %bitcast.57), calls=%async_computation.2 | async-start | bytes 6291456 | tf_op jit(solution)/shard_map/all_to_all | solution.py:81
  291.4 38.0 %all-to-all-start.1 = ((bf16[16,128,128]{2,1,0:T(8,128)(2,1)}), bf16[16,128,128]{2,1,0:T(8,128)(2,1)}, u32[]{:S(2)}, u32[]{:S(2)}) async-start(bf16[16,128,128]{2,1,0:T(8,128)(2,1)} %convert_element_type.40), calls=%async_computation.1 | async-start | bytes 1048576 | tf_op jit(solution)/shard_map/all_to_all | solution.py:59
  300.3 66.0 %reduce-scatter.3.cloned.1.call-start = ((), (), s32[]{:S(2)}) async-start(), calls=%async_computation.6 | async-start | bytes 4718592 | tf_op jit(solution)/shard_map/reduce_scatter | solution.py:33
  302.5 0.8 copy-start.2
  340.6 25.9 %copy-start.5 = (f32[256,2]{0,1:T(2,128)S(1)}, f32[256,2]{0,1:T(2,128)}, u32[]{:S(2)}) copy-start(f32[256,2]{0,1:T(2,128)} %param.9) | copy-start | bytes 6148
  340.6 25.9 %copy-start.4 = (s32[256,2]{0,1:T(2,128)S(1)}, s32[256,2]{0,1:T(2,128)}, u32[]{:S(2)}) copy-start(s32[256,2]{0,1:T(2,128)} %param.8) | copy-start | bytes 6148
  340.7 109.4 %reduce-scatter.5.cloned.1.call-start = ((), (), s32[]{:S(2)}) async-start(), calls=%async_computation.7 | async-start | bytes 1671168 | tf_op jit(solution)/shard_map/reduce_scatter | solution.py:33
  451.9 26.6 %all-to-all-start.3 = ((bf16[16,2,1536]{2,1,0:T(2,128)(2,1)}), bf16[16,2,1536]{2,1,0:T(2,128)(2,1)S(1)}, u32[]{:S(2)}, u32[]{:S(2)}) async-start(bf16[16,2,1536]{2,1,0:T(2,128)(2,1)} %reshape.76), calls=%async_computation.5 | async-start | bytes 196608 | tf_op jit(solution)/shard_map/all_to_all | solution.py:95
Sparse Core Ops, SparseCore 0:
  340.8 25.5 reduce-scatter.2
  369.8 80.2 reduce-scatter.4
where the time goes:
time: 489 us
  waiting for transfers between devices  323 us (66%)
  starting transfers between devices  114 us (23%)
  between operations  14.2 us (3%)
  local copies, waits for them, and re-layouts  13.2 us (3%)
  other arithmetic  12.8 us (3%)
  matrix products  11.1 us (2%)
    all_to_all x1, waiting for transfers between devices, on_device(): lax.all_to_all(outbound, 'fs', split_axis=0, concat_axis=0, tiled=True)  137 us
    reduce_scatter x2, waiting for transfers between devices, own_block(): tiles = lax.psum_scatter(tiles, axes[k], scatter_dimension=0, tiled=True)  109 us
    all_to_all x1, starting transfers between devices, side_by_side(): lax.all_to_all(both, axis, split_axis=split_dim, concat_axis=concat_dim,...  83.1 us
    all_to_all x1, waiting for transfers between devices, side_by_side(): lax.all_to_all(both, axis, split_axis=split_dim, concat_axis=concat_dim,...  42.2 us
    all_to_all x1, waiting for transfers between devices, on_device(): lax.all_to_all(rounded_down, 'fs', split_axis=0, concat_axis=1, tiled=True)  25.1 us
    all_to_all x1, starting transfers between devices, on_device(): lax.all_to_all(results, 'fs', split_axis=1, concat_axis=1, tiled=True)  13.8 us
    all_to_all x1, waiting for transfers between devices, on_device(): lax.all_to_all(results, 'fs', split_axis=1, concat_axis=1, tiled=True)  9.8 us
  transfers between devices with their start and end apart: 6, of which 6 were waited for; matrix products, arithmetic and copies ran while one was open for 3% of the time, Pallas kernels for 0%

commit v1 on v0

v1 whole, which is shorter than its diff:
```python
import functools

import jax
import jax.numpy as jnp
from jax import lax
from jax.experimental import pallas as pl
from jax.experimental.pallas import tpu as pltpu
from jax.sharding import PartitionSpec as P

EPS = 1e-06
MESH = pl.DeviceIdType.MESH
F32 = jnp.float32
BF16 = jnp.bfloat16


def loop(lo, hi, body):
    def step(i, carry):
        body(i)
        return carry

    lax.fori_loop(lo, hi, step, 0)


def kernel(
    dims,
    tokens_hbm,
    routes_ref,
    logits_ref,
    gain_ref,
    wg_hbm,
    wu_hbm,
    wd_hbm,
    go_hbm,
    uo_hbm,
    do_hbm,
    mix_ref,
    tok_v,
    normed_v,
    wf,
    wsend,
    wown,
    wpart,
    xb,
    dsend,
    pick,
    hid,
    acc_g,
    acc_u,
    part_r,
    part_l,
    rs_rsend,
    rs_lsend,
    rs_rrecv,
    rs_lrecv,
    ret_send,
    ret_recv,
    mix_own,
    mix_other,
    load_sem,
    store_sem,
    tok_s,
    tok_r,
    z_s,
    z_r,
    x_s,
    x_r,
    d_s,
    d_r,
    agr_s,
    agr_r,
    agl_s,
    agl_r,
    rsr_s,
    rsr_r,
    rsl_s,
    rsl_r,
    ret_s,
    ret_r,
    mix_s,
    mix_r,
):
    G, F, Y, cap, nsub = dims
    half = F // 2
    per = half // nsub
    right_steps, left_steps = Y // 2, Y // 2 - 1
    rows = wsend.shape[2]
    share = rows // G
    feats = xb.shape[3]

    g = lax.axis_index("grp")
    me = lax.axis_index("fs")
    t = lax.axis_index("tp")
    y = lax.div(t, 2)
    c = lax.rem(t, 2)
    partner = t + 1 - 2 * c
    right = lax.rem(y + 1, Y) * 2 + c
    left = lax.rem(y + Y - 1, Y) * 2 + c
    par = lax.rem(me + c, 2)

    def offset(m):
        step = lax.div(m + 1, 2)
        odd = lax.rem(m, 2)
        return odd * step + (1 - odd) * (F - step)

    barrier = pltpu.get_barrier_semaphore()

    def greet(m):
        pl.semaphore_signal(
            barrier, inc=1, device_id={"fs": lax.rem(me + m, F)}, device_id_type=MESH
        )

    loop(1, F, greet)
    for m in range(1, G):
        pl.semaphore_signal(
            barrier, inc=1, device_id={"grp": lax.rem(g + m, G)}, device_id_type=MESH
        )
    for other in (partner, left, right):
        pl.semaphore_signal(barrier, inc=1, device_id={"tp": other}, device_id_type=MESH)

    loads = [pltpu.make_async_copy(tokens_hbm, tok_v, load_sem.at[0])]
    for p, ref in enumerate((wg_hbm, wu_hbm, wd_hbm)):
        loads.append(pltpu.make_async_copy(ref, wf.at[p], load_sem.at[p + 1]))
    for copy in loads:
        copy.start()

    tok = tok_v.shape[0]
    lanes = 128
    experts = lax.broadcasted_iota(jnp.int32, (tok, lanes), 1)
    first = routes_ref[:, 0:1]
    second = routes_ref[:, 1:2]
    is_first = first == experts
    is_second = second == experts
    marked = jnp.where(is_first | is_second, 1.0, 0.0).astype(BF16)
    earlier = jnp.where(
        lax.broadcasted_iota(jnp.int32, (tok, tok), 1)
        < lax.broadcasted_iota(jnp.int32, (tok, tok), 0),
        1.0,
        0.0,
    ).astype(BF16)
    before = jnp.dot(earlier, marked, preferred_element_type=F32)
    key_first = first.astype(F32) * cap + jnp.sum(
        jnp.where(is_first, before, 0.0), axis=1, keepdims=True
    )
    key_second = second.astype(F32) * cap + jnp.sum(
        jnp.where(is_second, before, 0.0), axis=1, keepdims=True
    )
    place = lax.broadcasted_iota(jnp.int32, (1, half * cap), 1)
    ident = place + cap * par
    for k in range(1, half):
        ident = ident + jnp.where(place >= k * cap, cap, 0)
    ident = ident.astype(F32)
    pick[0] = jnp.where(key_first == ident, 1.0, 0.0).astype(BF16)
    pick[1] = jnp.where(key_second == ident, 1.0, 0.0).astype(BF16)

    loads[0].wait()
    chunk = 32

    def norm(i):
        at = pl.ds(pl.multiple_of(i * chunk, chunk), chunk)
        values = tok_v[at, :].astype(F32)
        mean = jnp.mean(values, axis=1, keepdims=True)
        centred = values - mean
        spread = jnp.mean(centred * centred, axis=1, keepdims=True)
        mine = tok_v[at, pl.ds(pl.multiple_of(y * feats, feats), feats)].astype(F32)
        normed_v[at, :] = ((mine - mean) * lax.rsqrt(spread + EPS)).astype(BF16)

    loop(0, tok // chunk, norm)
    picked = lax.dot_general(
        pick[0] + pick[1],
        normed_v[...],
        (((0,), (0,)), ((), ())),
        preferred_element_type=F32,
    )
    dsend[...] = picked.astype(BF16).reshape(dsend.shape)

    @pl.when(c == 0)
    def _():
        xb[y, lax.div(me, 2)] = dsend[lax.div(me, 2)]

    column = jnp.broadcast_to(gain_ref[...], (rows, rows)).T
    for copy in loads[1:]:
        copy.wait()

    def fold(e):
        wsend[e, 0] = (wf[0, e] * column).astype(BF16)
        wsend[e, 1] = (wf[1, e] * column).astype(BF16)
        wsend[e, 2] = wf[2, e].astype(BF16)

    loop(0, F, fold)
    for p in range(3):
        wown[p, me] = wsend[me, p]

    pl.semaphore_wait(barrier, F - 1 + G - 1 + 3)

    def tok_copy(k):
        return pltpu.make_async_remote_copy(
            src_ref=dsend.at[k],
            dst_ref=xb.at[y, lax.div(me, 2)],
            send_sem=tok_s.at[k],
            recv_sem=tok_r.at[lax.div(me, 2)],
            device_id={"fs": 2 * k + par},
            device_id_type=MESH,
        )

    def tok_arrival(k):
        return pltpu.make_async_remote_copy(
            src_ref=dsend.at[k],
            dst_ref=xb.at[y, k],
            send_sem=tok_s.at[k],
            recv_sem=tok_r.at[k],
            device_id={"fs": 2 * k + par},
            device_id_type=MESH,
        )

    def send_tok(m):
        k = lax.rem(lax.div(me, 2) + half // 2 + m, half)

        @pl.when(2 * k + par != me)
        def _():
            tok_copy(k).start()

    loop(0, half, send_tok)

    kinds = (pl.ds(0, 2), pl.ds(2, 1))
    mine = pl.ds(pl.multiple_of(g * share, share), share)

    def z_copy(kind, m):
        to = lax.rem(me + offset(m), F)
        return pltpu.make_async_remote_copy(
            src_ref=wsend.at[to, kinds[kind], mine],
            dst_ref=wown.at[kinds[kind], me, mine],
            send_sem=z_s.at[kind, m],
            recv_sem=z_r.at[kind, m],
            device_id={"fs": to},
            device_id_type=MESH,
        )

    def source(m):
        return lax.rem(me + F - offset(m), F)

    def x_copy(kind, m, n):
        at = wown.at[kinds[kind], source(m), mine]
        return pltpu.make_async_remote_copy(
            src_ref=at,
            dst_ref=at,
            send_sem=x_s.at[kind, n - 1, m],
            recv_sem=x_r.at[kind, n - 1, m],
            device_id={"grp": lax.rem(g + n, G)},
            device_id_type=MESH,
        )

    def d_copy(kind, m, s):
        return pltpu.make_async_remote_copy(
            src_ref=wown.at[kinds[kind], s],
            dst_ref=wpart.at[kinds[kind], s],
            send_sem=d_s.at[kind, m],
            recv_sem=d_r.at[kind, m],
            device_id={"tp": partner},
            device_id_type=MESH,
        )

    def pass_on(kind, m):
        z_copy(kind, m).wait_recv()
        for n in range(1, G):
            x_copy(kind, m, n).start()

    def hand_over(kind, m):
        for n in range(1, G):
            x_copy(kind, m, n).wait_recv()
        d_copy(kind, m, source(m)).start()

    for kind in (0, 1):
        loop(1, F, lambda m, kind=kind: z_copy(kind, m).start())
    for kind in (0, 1):
        d_copy(kind, 0, me).start()

    def ag_copy(i, j, to_right):
        blk = lax.rem(y + Y - i, Y) if to_right else lax.rem(y + i, Y)
        at = xb.at[blk, pl.ds(j * per, per)]
        return pltpu.make_async_remote_copy(
            src_ref=at,
            dst_ref=at,
            send_sem=(agr_s if to_right else agl_s).at[i, j],
            recv_sem=(agr_r if to_right else agl_r).at[i, j],
            device_id={"tp": right if to_right else left},
            device_id_type=MESH,
        )

    for j in range(nsub):
        for k in range(j * per, (j + 1) * per):

            @pl.when(2 * k + par != me)
            def _(k=k):
                tok_arrival(k).wait_recv()

        ag_copy(0, j, True).start()
        ag_copy(0, j, False).start()

    def ag_step(i, both):
        for j in range(nsub):
            ag_copy(i - 1, j, True).wait_recv()
            ag_copy(i, j, True).start()
            ag_copy(i - 1, j, False).wait_recv()
            if both:
                ag_copy(i, j, False).start()

    def forward(i):
        for m in (2 * i - 1, 2 * i):

            @pl.when(m < F)
            def _(m=m):
                pass_on(0, m)

    def settle(i):
        for m in (2 * i - 1, 2 * i):

            @pl.when(m < F)
            def _(m=m):
                hand_over(0, m)

    ag_step(1, 1 < left_steps)
    forward(1)

    def middle(i):
        ag_step(i, True)
        forward(i)
        settle(i - 1)

    loop(2, left_steps, middle)
    for i in range(max(2, left_steps), right_steps):
        ag_step(i, i < left_steps)
        forward(i)
        settle(i - 1)
    for j in range(nsub):
        ag_copy(right_steps - 1, j, True).wait_recv()
    settle(right_steps - 1)
    rest = min(F, 2 * right_steps - 1)
    loop(rest, F, lambda m: pass_on(0, m))
    loop(1, F // 2, lambda m: pass_on(1, m))
    loop(rest, F, lambda m: hand_over(0, m))
    loop(1, F // 2, lambda m: hand_over(1, m))
    loop(0, F, lambda m: d_copy(0, m, me).wait_recv())
    store_g = pltpu.make_async_copy(wown.at[0], go_hbm.at[0], store_sem.at[0])
    store_u = pltpu.make_async_copy(wown.at[1], uo_hbm.at[0], store_sem.at[1])
    store_g.start()
    store_u.start()

    acc_g[...] = jnp.zeros_like(acc_g)
    acc_u[...] = jnp.zeros_like(acc_u)
    area = half * cap

    def contract(m):
        lhs = jnp.concatenate(
            [xb[2 * m].reshape(area, feats), xb[2 * m + 1].reshape(area, feats)], axis=1
        )

        def rhs(p):
            top = jnp.concatenate([wown[p, 2 * m], wpart[p, 2 * m]], axis=1)
            low = jnp.concatenate([wown[p, 2 * m + 1], wpart[p, 2 * m + 1]], axis=1)
            return jnp.concatenate([top, low], axis=0)

        acc_g[...] += jnp.dot(lhs, rhs(0), preferred_element_type=F32)
        acc_u[...] += jnp.dot(lhs, rhs(1), preferred_element_type=F32)

    loop(0, Y // 2, contract)

    def activate(k):
        at = pl.ds(pl.multiple_of(k * cap, cap), cap)
        v = acc_g[at, :]
        hid[at, :] = (v / (1.0 + jnp.exp(-v)) * acc_u[at, :]).astype(BF16)

    loop(0, half, activate)

    loop(F // 2, F, lambda m: pass_on(1, m))
    loop(F // 2, F, lambda m: hand_over(1, m))
    loop(0, F, lambda m: d_copy(1, m, me).wait_recv())
    store_d = pltpu.make_async_copy(wown.at[2], do_hbm.at[0], store_sem.at[2])
    store_d.start()

    def product(d):
        block = jnp.concatenate([wown[2, d], wpart[2, d]], axis=1)
        return lax.dot_general(
            hid[...], block, (((1,), (1,)), ((), ())), preferred_element_type=F32
        )

    sub = per * cap

    def rs_copy(i, j, to_right):
        return pltpu.make_async_remote_copy(
            src_ref=(rs_rsend if to_right else rs_lsend).at[i, j],
            dst_ref=(rs_rrecv if to_right else rs_lrecv).at[i, j],
            send_sem=(rsr_s if to_right else rsl_s).at[i, j],
            recv_sem=(rsr_r if to_right else rsl_r).at[i, j],
            device_id={"tp": right if to_right else left},
            device_id_type=MESH,
        )

    def right_chunk(i):
        return lax.rem(y + right_steps + Y - i, Y)

    def left_chunk(i):
        return lax.rem(y + Y - left_steps + i, Y)

    part_r[...] = product(right_chunk(0))
    for j in range(nsub):
        rs_rsend[0, j] = part_r[pl.ds(j * sub, sub), :].astype(BF16)
        rs_copy(0, j, True).start()
    part_l[...] = product(left_chunk(0))
    for j in range(nsub):
        rs_lsend[0, j] = part_l[pl.ds(j * sub, sub), :].astype(BF16)
        rs_copy(0, j, False).start()

    def rs_step(i, both):
        part_r[...] = product(right_chunk(i))
        if both:
            part_l[...] = product(left_chunk(i))
        for j in range(nsub):
            at = pl.ds(j * sub, sub)
            rs_copy(i - 1, j, True).wait_recv()
            rs_rsend[i, j] = (rs_rrecv[i - 1, j].astype(F32) + part_r[at, :]).astype(BF16)
            rs_copy(i, j, True).start()
            if both:
                rs_copy(i - 1, j, False).wait_recv()
                rs_lsend[i, j] = (rs_lrecv[i - 1, j].astype(F32) + part_l[at, :]).astype(BF16)
                rs_copy(i, j, False).start()

    loop(1, left_steps, lambda i: rs_step(i, True))
    for i in range(max(1, left_steps), right_steps):
        rs_step(i, False)

    def ret_copy(k):
        return pltpu.make_async_remote_copy(
            src_ref=ret_send.at[k],
            dst_ref=ret_recv.at[lax.div(me, 2)],
            send_sem=ret_s.at[k],
            recv_sem=ret_r.at[lax.div(me, 2)],
            device_id={"fs": 2 * k + par},
            device_id_type=MESH,
        )

    def ret_arrival(k):
        return pltpu.make_async_remote_copy(
            src_ref=ret_send.at[k],
            dst_ref=ret_recv.at[k],
            send_sem=ret_s.at[k],
            recv_sem=ret_r.at[k],
            device_id={"fs": 2 * k + par},
            device_id_type=MESH,
        )

    part_r[...] = product(y)
    for j in range(nsub):
        rs_copy(left_steps - 1, j, False).wait_recv()
        rs_copy(right_steps - 1, j, True).wait_recv()
        total = (
            part_r[pl.ds(j * sub, sub), :]
            + rs_rrecv[right_steps - 1, j].astype(F32)
            + rs_lrecv[left_steps - 1, j].astype(F32)
        ).astype(BF16)
        ret_send[pl.ds(j * per, per)] = total.reshape(per, cap, feats)
        for k in range(j * per, (j + 1) * per):

            @pl.when(2 * k + par != me)
            def _(k=k):
                ret_copy(k).start()

    @pl.when(c == 0)
    def _():
        ret_recv[lax.div(me, 2)] = ret_send[lax.div(me, 2)]

    diff = logits_ref[:, 0:1] - logits_ref[:, 1:2]
    share_first = 1.0 / (1.0 + jnp.exp(-diff))
    share_second = 1.0 / (1.0 + jnp.exp(diff))

    for k in range(half):

        @pl.when(2 * k + par != me)
        def _(k=k):
            ret_arrival(k).wait_recv()

    returned = ret_recv[...].reshape(area, feats)
    mix_own[...] = share_first * jnp.dot(
        pick[0], returned, preferred_element_type=F32
    ) + share_second * jnp.dot(pick[1], returned, preferred_element_type=F32)
    swap = pltpu.make_async_remote_copy(
        src_ref=mix_own,
        dst_ref=mix_other,
        send_sem=mix_s,
        recv_sem=mix_r,
        device_id={"tp": partner},
        device_id_type=MESH,
    )
    swap.start()
    swap.wait_recv()
    both = mix_own[...] + mix_other[...]
    width = mix_ref.shape[1]
    mix_ref[...] = jnp.where(c == 0, both[:, :width], both[:, width:]).astype(BF16)

    swap.wait_send()
    for copy in (store_g, store_u, store_d):
        copy.wait()

    def drain_tok(k):
        @pl.when(2 * k + par != me)
        def _():
            tok_copy(k).wait_send()
            ret_copy(k).wait_send()

    loop(0, half, drain_tok)
    for kind in (0, 1):

        def drain(m, kind=kind):
            z_copy(kind, m).wait_send()
            for n in range(1, G):
                x_copy(kind, m, n).wait_send()

        loop(1, F, drain)
        loop(0, F, lambda m, kind=kind: d_copy(kind, m, me).wait_send())

    def drain_ring(i):
        for j in range(nsub):
            ag_copy(i, j, True).wait_send()
            rs_copy(i, j, True).wait_send()

    def drain_ring_left(i):
        for j in range(nsub):
            ag_copy(i, j, False).wait_send()
            rs_copy(i, j, False).wait_send()

    loop(0, right_steps, drain_ring)
    loop(0, left_steps, drain_ring_left)


def solution(mesh):
    G, F, Y = mesh.shape["grp"], mesh.shape["fs"], mesh.shape["tp"] // 2

    def on_device(tokens, routes, route_logits, gain, w_gate, w_up, w_down):
        experts, rows, cols = w_gate.shape
        tok, width = tokens.shape
        cap = 3 * tok // experts
        half = F // 2
        nsub = min(4, half)
        feats = width // Y
        area = half * cap
        rs, ls = Y // 2, Y // 2 - 1
        any_spec = pl.BlockSpec(memory_space=pl.ANY)
        vmem = pl.BlockSpec(memory_space=pltpu.VMEM)
        dma = pltpu.SemaphoreType.DMA
        out = jax.ShapeDtypeStruct((1, F, rows, cols), BF16)
        gate_out, up_out, down_out, mixed = pl.pallas_call(
            functools.partial(kernel, (G, F, Y, cap, nsub)),
            out_shape=(out, out, out, jax.ShapeDtypeStruct((tok, feats // 2), BF16)),
            in_specs=[any_spec, vmem, vmem, vmem, any_spec, any_spec, any_spec],
            out_specs=(any_spec, any_spec, any_spec, vmem),
            scratch_shapes=[
                pltpu.VMEM((tok, width), BF16),
                pltpu.VMEM((tok, feats), BF16),
                pltpu.VMEM((3, F, rows, cols), F32),
                pltpu.VMEM((F, 3, rows, cols), BF16),
                pltpu.VMEM((3, F, rows, cols), BF16),
                pltpu.VMEM((3, F, rows, cols), BF16),
                pltpu.VMEM((Y, half, cap, feats), BF16),
                pltpu.VMEM((half, cap, feats), BF16),
                pltpu.VMEM((2, tok, area), BF16),
                pltpu.VMEM((area, 2 * cols), BF16),
                pltpu.VMEM((area, 2 * cols), F32),
                pltpu.VMEM((area, 2 * cols), F32),
                pltpu.VMEM((area, feats), F32),
                pltpu.VMEM((area, feats), F32),
                pltpu.VMEM((rs, nsub, area // nsub, feats), BF16),
                pltpu.VMEM((ls, nsub, area // nsub, feats), BF16),
                pltpu.VMEM((rs, nsub, area // nsub, feats), BF16),
                pltpu.VMEM((ls, nsub, area // nsub, feats), BF16),
                pltpu.VMEM((half, cap, feats), BF16),
                pltpu.VMEM((half, cap, feats), BF16),
                pltpu.VMEM((tok, feats), F32),
                pltpu.VMEM((tok, feats), F32),
                dma((4,)),
                dma((3,)),
                dma((half,)),
                dma((half,)),
                dma((2, F)),
                dma((2, F)),
                dma((2, max(G - 1, 1), F)),
                dma((2, max(G - 1, 1), F)),
                dma((2, F)),
                dma((2, F)),
                dma((rs, nsub)),
                dma((rs, nsub)),
                dma((ls, nsub)),
                dma((ls, nsub)),
                dma((rs, nsub)),
                dma((rs, nsub)),
                dma((ls, nsub)),
                dma((ls, nsub)),
                dma((half,)),
                dma((half,)),
                dma,
                dma,
            ],
            compiler_params=pltpu.CompilerParams(collective_id=0, has_side_effects=True),
        )(tokens, routes, route_logits, gain.reshape(1, rows), w_gate, w_up, w_down)
        weights = tuple(w.reshape(1, F * rows, cols) for w in (gate_out, up_out, down_out))
        return (*weights, mixed)

    in_specs = (
        P(("grp", "fs"), None),
        P(("grp", "fs"), None),
        P(("grp", "fs"), None),
        P("fs"),
        P(None, "fs", "tp"),
        P(None, "fs", "tp"),
        P(None, "fs", "tp"),
    )
    out_specs = (
        P(("grp", "fs"), None, "tp"),
        P(("grp", "fs"), None, "tp"),
        P(("grp", "fs"), None, "tp"),
        P(("grp", "fs"), "tp"),
    )
    return jax.shard_map(
        on_device, mesh=mesh, in_specs=in_specs, out_specs=out_specs, check_vma=False
    )
```

time: 489 us -> 190 us (0.39)
  waiting for transfers between devices: 323 us -> 0 us
  Pallas kernels: 0 us -> 179 us
  starting transfers between devices: 114 us -> 0 us
  between operations: 14.2 us -> 0.65 us
  other arithmetic: 12.8 us -> 0 us
  matrix products: 11.1 us -> 0 us
  local copies, waits for them, and re-layouts: 13.2 us -> 7.78 us
    all_to_all x4 -> x0, waiting for transfers between devices: 214 us -> none  [the longest x1 137 us: on_device(): lax.all_to_all(outbound, 'fs', split_axis=0, concat_axis=0, tiled=True)]
    pallas_call x0 -> x1, Pallas kernels: none -> 179 us  [on_device(): pl.pallas_call(functools.partial(kernel, (G, F, Y, cap, nsub)), out_shape...]
    all_to_all x4 -> x0, starting transfers between devices: 114 us -> none  [the longest x1 83.1 us: side_by_side(): lax.all_to_all(both, axis, split_axis=split_dim, concat_axis=concat_dim,...]
    reduce_scatter x2 -> x0, waiting for transfers between devices: 109 us -> none  [own_block(): tiles = lax.psum_scatter(tiles, axes[k], scatter_dimension=0, tiled=True)]
    dot_general x4 -> x0, matrix products: 11.1 us -> none  [the longest x1 6.19 us: on_device(): lax.dot_general(down_local, hidden, (((1,), (1,)), ((), ())), preferred_e...]
  transfers between devices with their start and end apart: 6 -> 0, of which waited for: 6 -> 0; matrix products, arithmetic and copies ran while one was open for 3% -> 0% of each run, Pallas kernels for 0% -> 0%
where the time goes in v1:
time: 190 us; the launch traced here: 187 us
  Pallas kernels  179 us (94%)
  local copies, waits for them, and re-layouts  7.78 us (4%)
    pallas_call x1, Pallas kernels, on_device(): pl.pallas_call(functools.partial(kernel, (G, F, Y, cap, nsub)), out_shape...  179 us
    unnamed x12, local copies, waits for them, and re-layouts  7.78 us

profile of v1, /device:TPU:6, one launch (start us, length us, event | category | flops | bytes accessed | tf_op | source)
XLA Modules:
  0.0 187.3 jit_solution(11914865454658899449)
XLA Ops:
  0.6 0.0 copy-start.2
  0.6 1.5 copy.11.routes_ref
  2.1 0.0 copy-done.2
  2.1 0.8 copy.12.logits_ref
  2.9 178.8 %shard_map.102 = (bf16[1,16,128,128]{3,2,1,0:T(8,128)(2,1)}, bf16[1,16,128,128]{3,2,1,0:T(8,128)(2,1)}, bf16[1,16,128,128]{3,2,1,0:T(8,128)(2,1)}, bf16[256,64]{1,0:T(8,128)(2,1)}) custom-call(bf16[256,2048]{1,0:T(8,128)(2,1)} %tokens_hbm.1, s32[256,2]{1,0:T(8,128)} %copy.11.routes_ref, f32[256,2]{1,0:T(8,128)} %copy.12.logits_ref, f32[1,128]{1,0:T(1,128)} %bitcast.7, ...), custom_call_target="tpu_custom_call" | custom-call | tf_op jit(solution)/shard_map/pallas_call | solution.py:550
  181.8 1.5 copy.13
  183.3 0.0 copy-start.1
  183.3 1.9 %copy.17 = bf16[1,2048,128]{2,1,0:T(8,128)(2,1)} copy(bf16[1,2048,128]{2,1,0:T(8,128)(2,1)} %bitcast.6) | data formatting | bytes 1048576
  185.2 0.0 copy-done.1
  185.2 0.0 copy-start
  185.3 0.8 copy.18
  186.0 0.4 copy-done
  186.5 0.8 copy.19
Async XLA Ops:
  0.6 1.5 copy-start.2
  183.3 1.9 %copy-start.1 = (bf16[1,16,128,128]{3,2,1,0:T(8,128)(2,1)S(1)}, bf16[1,16,128,128]{3,2,1,0:T(8,128)(2,1)}, u32[]{:S(2)}) copy-start(bf16[1,16,128,128]{3,2,1,0:T(8,128)(2,1)} %get-tuple-element.9) | copy-start | bytes 1572868
  185.2 1.2 copy-start

commit v2 on v1

--- a/solution.py
+++ b/solution.py
@@ -54,6 +54,7 @@
     rs_lrecv,
     ret_send,
     ret_recv,
+    share_tab,
     mix_own,
     mix_other,
     load_sem,
@@ -97,6 +98,9 @@
     left = lax.rem(y + Y - 1, Y) * 2 + c
     par = lax.rem(me + c, 2)
 
+    def taken(sem, refs):
+        pltpu.make_async_copy(refs, refs, sem).wait()
+
     def offset(m):
         step = lax.div(m + 1, 2)
         odd = lax.rem(m, 2)
@@ -125,9 +129,19 @@
 
     tok = tok_v.shape[0]
     lanes = 128
-    experts = lax.broadcasted_iota(jnp.int32, (tok, lanes), 1)
-    first = routes_ref[:, 0:1]
-    second = routes_ref[:, 1:2]
+    experts = lax.broadcasted_iota(jnp.int32, (tok, lanes), 1).astype(F32)
+    line = lax.broadcasted_iota(jnp.int32, (8, tok), 0)
+    table = jnp.where(
+        line == 0,
+        routes_ref[0:1, :].astype(F32),
+        jnp.where(
+            line == 1,
+            routes_ref[1:2, :].astype(F32),
+            jnp.where(line == 2, logits_ref[0:1, :], logits_ref[1:2, :]),
+        ),
+    ).T
+    first = table[:, 0:1]
+    second = table[:, 1:2]
     is_first = first == experts
     is_second = second == experts
     marked = jnp.where(is_first | is_second, 1.0, 0.0).astype(BF16)
@@ -138,10 +152,10 @@
         0.0,
     ).astype(BF16)
     before = jnp.dot(earlier, marked, preferred_element_type=F32)
-    key_first = first.astype(F32) * cap + jnp.sum(
+    key_first = first * cap + jnp.sum(
         jnp.where(is_first, before, 0.0), axis=1, keepdims=True
     )
-    key_second = second.astype(F32) * cap + jnp.sum(
+    key_second = second * cap + jnp.sum(
         jnp.where(is_second, before, 0.0), axis=1, keepdims=True
     )
     place = lax.broadcasted_iota(jnp.int32, (1, half * cap), 1)
@@ -152,6 +166,10 @@
     pick[0] = jnp.where(key_first == ident, 1.0, 0.0).astype(BF16)
     pick[1] = jnp.where(key_second == ident, 1.0, 0.0).astype(BF16)
 
+    diff = table[:, 2:3] - table[:, 3:4]
+    share_tab[0] = jnp.broadcast_to(1.0 / (1.0 + jnp.exp(-diff)), (tok, lanes))
+    share_tab[1] = jnp.broadcast_to(1.0 / (1.0 + jnp.exp(diff)), (tok, lanes))
+
     loads[0].wait()
     chunk = 32
 
@@ -196,7 +214,7 @@
         return pltpu.make_async_remote_copy(
             src_ref=dsend.at[k],
             dst_ref=xb.at[y, lax.div(me, 2)],
-            send_sem=tok_s.at[k],
+            send_sem=tok_s,
             recv_sem=tok_r.at[lax.div(me, 2)],
             device_id={"fs": 2 * k + par},
             device_id_type=MESH,
@@ -206,11 +224,60 @@
         return pltpu.make_async_remote_copy(
             src_ref=dsend.at[k],
             dst_ref=xb.at[y, k],
-            send_sem=tok_s.at[k],
+            send_sem=tok_s,
             recv_sem=tok_r.at[k],
             device_id={"fs": 2 * k + par},
             device_id_type=MESH,
         )
+
+    kinds = (pl.ds(0, 2), pl.ds(2, 1))
+    mine = pl.ds(pl.multiple_of(g * share, share), share)
+
+    def z_copy(kind, to, source):
+        return pltpu.make_async_remote_copy(
+            src_ref=wsend.at[to, kinds[kind], mine],
+            dst_ref=wown.at[kinds[kind], source, mine],
+            send_sem=z_s,
+            recv_sem=z_r.at[kind, source],
+            device_id={"fs": to},
+            device_id_type=MESH,
+        )
+
+    def x_copy(kind, s, n):
+        at = wown.at[kinds[kind], s, mine]
+        return pltpu.make_async_remote_copy(
+            src_ref=at,
+            dst_ref=at,
+            send_sem=x_s.at[n - 1],
+            recv_sem=x_r.at[kind, n - 1, s],
+            device_id={"grp": lax.rem(g + n, G)},
+            device_id_type=MESH,
+        )
+
+    def d_copy(kind, s):
+        return pltpu.make_async_remote_copy(
+            src_ref=wown.at[kinds[kind], s],
+            dst_ref=wpart.at[kinds[kind], s],
+            send_sem=d_s,
+            recv_sem=d_r.at[kind * (s + 1)],
+            device_id={"tp": partner},
+            device_id_type=MESH,
+        )
+
+    def pass_on(kind, s):
+        z_copy(kind, s, s).wait_recv()
+        for n in range(1, G):
+            x_copy(kind, s, n).start()
+
+    def hand_over(kind, s):
+        for n in range(1, G):
+            x_copy(kind, s, n).wait_recv()
+        d_copy(kind, s).start()
+
+    def send_tok(k):
+        @pl.when(lax.rem(k, 2) == par)
+        def _():
+            tok_copy(lax.div(k, 2)).start()
 
     def send_tok(m):
         k = lax.rem(lax.div(me, 2) + half // 2 + m, half)
@@ -220,59 +287,22 @@
             tok_copy(k).start()
 
     loop(0, half, send_tok)
-
-    kinds = (pl.ds(0, 2), pl.ds(2, 1))
-    mine = pl.ds(pl.multiple_of(g * share, share), share)
-
-    def z_copy(kind, m):
-        to = lax.rem(me + offset(m), F)
-        return pltpu.make_async_remote_copy(
-            src_ref=wsend.at[to, kinds[kind], mine],
-            dst_ref=wown.at[kinds[kind], me, mine],
-            send_sem=z_s.at[kind, m],
-            recv_sem=z_r.at[kind, m],
-            device_id={"fs": to},
-            device_id_type=MESH,
-        )
+    def send_weights(kind):
+        loop(1, F, lambda m: z_copy(kind, lax.rem(me + offset(m), F), me).start())
+
+    ahead = lax.rem(me + F - y, F)
+    soon = (ahead >= F // 4 + 1) & (ahead <= F - F // 4)
+    send_weights(0)
+
+    @pl.when(soon)
+    def _():
+        send_weights(1)
+
+    for kind in (0, 1):
+        d_copy(kind, me).start()
 
     def source(m):
         return lax.rem(me + F - offset(m), F)
-
-    def x_copy(kind, m, n):
-        at = wown.at[kinds[kind], source(m), mine]
-        return pltpu.make_async_remote_copy(
-            src_ref=at,
-            dst_ref=at,
-            send_sem=x_s.at[kind, n - 1, m],
-            recv_sem=x_r.at[kind, n - 1, m],
-            device_id={"grp": lax.rem(g + n, G)},
-            device_id_type=MESH,
-        )
-
-    def d_copy(kind, m, s):
-        return pltpu.make_async_remote_copy(
-            src_ref=wown.at[kinds[kind], s],
-            dst_ref=wpart.at[kinds[kind], s],
-            send_sem=d_s.at[kind, m],
-            recv_sem=d_r.at[kind, m],
-            device_id={"tp": partner},
-            device_id_type=MESH,
-        )
-
-    def pass_on(kind, m):
-        z_copy(kind, m).wait_recv()
-        for n in range(1, G):
-            x_copy(kind, m, n).start()
-
-    def hand_over(kind, m):
-        for n in range(1, G):
-            x_copy(kind, m, n).wait_recv()
-        d_copy(kind, m, source(m)).start()
-
-    for kind in (0, 1):
-        loop(1, F, lambda m, kind=kind: z_copy(kind, m).start())
-    for kind in (0, 1):
-        d_copy(kind, 0, me).start()
 
     def ag_copy(i, j, to_right):
         blk = lax.rem(y + Y - i, Y) if to_right else lax.rem(y + i, Y)
@@ -280,7 +310,7 @@
         return pltpu.make_async_remote_copy(
             src_ref=at,
             dst_ref=at,
-            send_sem=(agr_s if to_right else agl_s).at[i, j],
+            send_sem=agr_s if to_right else agl_s,
             recv_sem=(agr_r if to_right else agl_r).at[i, j],
             device_id={"tp": right if to_right else left},
             device_id_type=MESH,
@@ -304,42 +334,32 @@
             if both:
                 ag_copy(i, j, False).start()
 
-    def forward(i):
+    def forward(act, kind, i):
         for m in (2 * i - 1, 2 * i):
 
-            @pl.when(m < F)
+            @pl.when((m > 0) & (m < F))
             def _(m=m):
-                pass_on(0, m)
-
-    def settle(i):
-        for m in (2 * i - 1, 2 * i):
-
-            @pl.when(m < F)
-            def _(m=m):
-                hand_over(0, m)
-
-    ag_step(1, 1 < left_steps)
-    forward(1)
+                act(kind, source(m))
+
+    def tend(i):
+        forward(pass_on, 0, i)
+        forward(hand_over, 0, i - 1)
 
     def middle(i):
         ag_step(i, True)
-        forward(i)
-        settle(i - 1)
-
-    loop(2, left_steps, middle)
-    for i in range(max(2, left_steps), right_steps):
+        tend(i)
+
+    loop(1, left_steps, middle)
+    for i in range(left_steps, right_steps):
         ag_step(i, i < left_steps)
-        forward(i)
-        settle(i - 1)
-    for j in range(nsub):
-        ag_copy(right_steps - 1, j, True).wait_recv()
-    settle(right_steps - 1)
-    rest = min(F, 2 * right_steps - 1)
-    loop(rest, F, lambda m: pass_on(0, m))
-    loop(1, F // 2, lambda m: pass_on(1, m))
-    loop(rest, F, lambda m: hand_over(0, m))
-    loop(1, F // 2, lambda m: hand_over(1, m))
-    loop(0, F, lambda m: d_copy(0, m, me).wait_recv())
+        tend(i)
+
+    @pl.when(jnp.logical_not(soon))
+    def _():
+        send_weights(1)
+
+    loop(right_steps, F // 2 + 2, tend)
+    taken(d_r.at[0], wpart.at[kinds[0]])
     store_g = pltpu.make_async_copy(wown.at[0], go_hbm.at[0], store_sem.at[0])
     store_u = pltpu.make_async_copy(wown.at[1], uo_hbm.at[0], store_sem.at[1])
     store_g.start()
@@ -349,20 +369,23 @@
     acc_u[...] = jnp.zeros_like(acc_u)
     area = half * cap
 
-    def contract(m):
+    def contract(a, b):
         lhs = jnp.concatenate(
-            [xb[2 * m].reshape(area, feats), xb[2 * m + 1].reshape(area, feats)], axis=1
+            [xb[a].reshape(area, feats), xb[b].reshape(area, feats)], axis=1
         )
 
         def rhs(p):
-            top = jnp.concatenate([wown[p, 2 * m], wpart[p, 2 * m]], axis=1)
-            low = jnp.concatenate([wown[p, 2 * m + 1], wpart[p, 2 * m + 1]], axis=1)
+            top = jnp.concatenate([wown[p, a], wpart[p, a]], axis=1)
+            low = jnp.concatenate([wown[p, b], wpart[p, b]], axis=1)
             return jnp.concatenate([top, low], axis=0)
 
         acc_g[...] += jnp.dot(lhs, rhs(0), preferred_element_type=F32)
         acc_u[...] += jnp.dot(lhs, rhs(1), preferred_element_type=F32)
 
-    loop(0, Y // 2, contract)
+    loop(1, left_steps + 1, lambda i: contract(lax.rem(y + Y - i, Y), lax.rem(y + i, Y)))
+    for j in range(nsub):
+        ag_copy(right_steps - 1, j, True).wait_recv()
+    contract(y, lax.rem(y + right_steps, Y))
 
     def activate(k):
         at = pl.ds(pl.multiple_of(k * cap, cap), cap)
@@ -371,12 +394,6 @@
 
     loop(0, half, activate)
 
-    loop(F // 2, F, lambda m: pass_on(1, m))
-    loop(F // 2, F, lambda m: hand_over(1, m))
-    loop(0, F, lambda m: d_copy(1, m, me).wait_recv())
-    store_d = pltpu.make_async_copy(wown.at[2], do_hbm.at[0], store_sem.at[2])
-    store_d.start()
-
     def product(d):
         block = jnp.concatenate([wown[2, d], wpart[2, d]], axis=1)
         return lax.dot_general(
@@ -389,7 +406,7 @@
         return pltpu.make_async_remote_copy(
             src_ref=(rs_rsend if to_right else rs_lsend).at[i, j],
             dst_ref=(rs_rrecv if to_right else rs_lrecv).at[i, j],
-            send_sem=(rsr_s if to_right else rsl_s).at[i, j],
+            send_sem=rsr_s if to_right else rsl_s,
             recv_sem=(rsr_r if to_right else rsl_r).at[i, j],
             device_id={"tp": right if to_right else left},
             device_id_type=MESH,
@@ -401,6 +418,32 @@
     def left_chunk(i):
         return lax.rem(y + Y - left_steps + i, Y)
 
+    def chunk_of(n):
+        i = lax.div(n, 2)
+        odd = lax.rem(n, 2)
+        return lax.rem(y + Y + (1 - odd) * (right_steps - i) + odd * (i - left_steps), Y)
+
+    def down_block(act, n):
+        s = chunk_of(n)
+
+        @pl.when((n < F) & (s != me))
+        def _():
+            act(1, s)
+
+    def down_ready(i, both=True):
+        for n in (2 * i + 4, 2 * i + 5):
+            down_block(pass_on, n)
+        for n in (2 * i + 2, 2 * i + 3):
+            down_block(hand_over, n)
+        d_copy(1, chunk_of(2 * i)).wait_recv()
+        if both:
+            d_copy(1, chunk_of(2 * i + 1)).wait_recv()
+
+    for n in range(4):
+        down_block(pass_on, n)
+    for n in range(2):
+        down_block(hand_over, n)
+    down_ready(0)
     part_r[...] = product(right_chunk(0))
     for j in range(nsub):
         rs_rsend[0, j] = part_r[pl.ds(j * sub, sub), :].astype(BF16)
@@ -411,6 +454,7 @@
         rs_copy(0, j, False).start()
 
     def rs_step(i, both):
+        down_ready(i)
         part_r[...] = product(right_chunk(i))
         if both:
             part_l[...] = product(left_chunk(i))
@@ -432,22 +476,14 @@
         return pltpu.make_async_remote_copy(
             src_ref=ret_send.at[k],
             dst_ref=ret_recv.at[lax.div(me, 2)],
-            send_sem=ret_s.at[k],
-            recv_sem=ret_r.at[lax.div(me, 2)],
+            send_sem=ret_s,
+            recv_sem=ret_r,
             device_id={"fs": 2 * k + par},
             device_id_type=MESH,
         )
 
-    def ret_arrival(k):
-        return pltpu.make_async_remote_copy(
-            src_ref=ret_send.at[k],
-            dst_ref=ret_recv.at[k],
-            send_sem=ret_s.at[k],
-            recv_sem=ret_r.at[k],
-            device_id={"fs": 2 * k + par},
-            device_id_type=MESH,
-        )
-
+    store_d = pltpu.make_async_copy(wown.at[2], do_hbm.at[0], store_sem.at[2])
+    store_d.start()
     part_r[...] = product(y)
     for j in range(nsub):
         rs_copy(left_steps - 1, j, False).wait_recv()
@@ -468,20 +504,20 @@
     def _():
         ret_recv[lax.div(me, 2)] = ret_send[lax.div(me, 2)]
 
-    diff = logits_ref[:, 0:1] - logits_ref[:, 1:2]
-    share_first = 1.0 / (1.0 + jnp.exp(-diff))
-    share_second = 1.0 / (1.0 + jnp.exp(diff))
-
-    for k in range(half):
-
-        @pl.when(2 * k + par != me)
-        def _(k=k):
-            ret_arrival(k).wait_recv()
-
+    def all_but_own(sem, ref):
+        @pl.when(c == 0)
+        def _():
+            taken(sem, ref.at[pl.ds(0, half - 1)])
+
+        @pl.when(c == 1)
+        def _():
+            taken(sem, ref)
+
+    all_but_own(ret_r, ret_recv)
     returned = ret_recv[...].reshape(area, feats)
-    mix_own[...] = share_first * jnp.dot(
+    mix_own[...] = share_tab[0] * jnp.dot(
         pick[0], returned, preferred_element_type=F32
-    ) + share_second * jnp.dot(pick[1], returned, preferred_element_type=F32)
+    ) + share_tab[1] * jnp.dot(pick[1], returned, preferred_element_type=F32)
     swap = pltpu.make_async_remote_copy(
         src_ref=mix_own,
         dst_ref=mix_other,
@@ -492,43 +528,37 @@
     )
     swap.start()
     swap.wait_recv()
-    both = mix_own[...] + mix_other[...]
-    width = mix_ref.shape[1]
-    mix_ref[...] = jnp.where(c == 0, both[:, :width], both[:, width:]).astype(BF16)
+    both = (mix_own[...] + mix_other[...]).T
+    width = mix_ref.shape[0]
+    mix_ref[...] = jnp.where(c == 0, both[:width, :], both[width:, :]).astype(BF16)
 
     swap.wait_send()
     for copy in (store_g, store_u, store_d):
         copy.wait()
 
-    def drain_tok(k):
-        @pl.when(2 * k + par != me)
-        def _():
-            tok_copy(k).wait_send()
-            ret_copy(k).wait_send()
-
-    loop(0, half, drain_tok)
-    for kind in (0, 1):
-
-        def drain(m, kind=kind):
-            z_copy(kind, m).wait_send()
-            for n in range(1, G):
-                x_copy(kind, m, n).wait_send()
-
-        loop(1, F, drain)
-        loop(0, F, lambda m, kind=kind: d_copy(kind, m, me).wait_send())
-
-    def drain_ring(i):
-        for j in range(nsub):
-            ag_copy(i, j, True).wait_send()
-            rs_copy(i, j, True).wait_send()
-
-    def drain_ring_left(i):
-        for j in range(nsub):
-            ag_copy(i, j, False).wait_send()
-            rs_copy(i, j, False).wait_send()
-
-    loop(0, right_steps, drain_ring)
-    loop(0, left_steps, drain_ring_left)
+    all_but_own(tok_s, dsend)
+    all_but_own(ret_s, ret_send)
+    taken(z_s, wsend.at[pl.ds(0, F - 1), :, mine])
+    for n in range(1, G):
+        taken(x_s.at[n - 1], wown.at[:, pl.ds(0, F - 1), mine])
+    taken(d_s, wown)
+    taken(agr_s, xb.at[pl.ds(0, right_steps)])
+    taken(agl_s, xb.at[pl.ds(0, left_steps)])
+    taken(rsr_s, rs_rsend)
+    taken(rsl_s, rs_lsend)
+
+
+def hand_in(n, *refs):
+    sources, results, holds, sems = refs[:n], refs[n : 2 * n], refs[2 * n : 3 * n], refs[3 * n]
+    ins = [pltpu.make_async_copy(sources[i], holds[i], sems.at[0, i]) for i in range(n)]
+    outs = [pltpu.make_async_copy(holds[i], results[i], sems.at[1, i]) for i in range(n)]
+    for copy in ins:
+        copy.start()
+    for i in range(n):
+        ins[i].wait()
+        outs[i].start()
+    for copy in outs:
+        copy.wait()
 
 
 def solution(mesh):
@@ -547,9 +577,9 @@
         vmem = pl.BlockSpec(memory_space=pltpu.VMEM)
         dma = pltpu.SemaphoreType.DMA
         out = jax.ShapeDtypeStruct((1, F, rows, cols), BF16)
-        gate_out, up_out, down_out, mixed = pl.pallas_call(
+        made = pl.pallas_call(
             functools.partial(kernel, (G, F, Y, cap, nsub)),
-            out_shape=(out, out, out, jax.ShapeDtypeStruct((tok, feats // 2), BF16)),
+            out_shape=(out, out, out, jax.ShapeDtypeStruct((feats // 2, tok), BF16)),
             in_specs=[any_spec, vmem, vmem, vmem, any_spec, any_spec, any_spec],
             out_specs=(any_spec, any_spec, any_spec, vmem),
             scratch_shapes=[
@@ -573,35 +603,43 @@
                 pltpu.VMEM((ls, nsub, area // nsub, feats), BF16),
                 pltpu.VMEM((half, cap, feats), BF16),
                 pltpu.VMEM((half, cap, feats), BF16),
+                pltpu.VMEM((2, tok, feats), F32),
                 pltpu.VMEM((tok, feats), F32),
                 pltpu.VMEM((tok, feats), F32),
                 dma((4,)),
                 dma((3,)),
+                dma,
                 dma((half,)),
-                dma((half,)),
+                dma,
                 dma((2, F)),
-                dma((2, F)),
+                dma((max(G - 1, 1),)),
                 dma((2, max(G - 1, 1), F)),
-                dma((2, max(G - 1, 1), F)),
-                dma((2, F)),
-                dma((2, F)),
+                dma,
+                dma((F + 1,)),
+                dma,
                 dma((rs, nsub)),
+                dma,
+                dma((ls, nsub)),
+                dma,
                 dma((rs, nsub)),
+                dma,
                 dma((ls, nsub)),
-                dma((ls, nsub)),
-                dma((rs, nsub)),
-                dma((rs, nsub)),
-                dma((ls, nsub)),
-                dma((ls, nsub)),
-                dma((half,)),
-                dma((half,)),
+                dma,
+                dma,
                 dma,
                 dma,
             ],
             compiler_params=pltpu.CompilerParams(collective_id=0, has_side_effects=True),
-        )(tokens, routes, route_logits, gain.reshape(1, rows), w_gate, w_up, w_down)
+        )(tokens, routes.T, route_logits.T, gain.reshape(1, rows), w_gate, w_up, w_down)
+        gate_out, up_out, down_out, mixed = pl.pallas_call(
+            functools.partial(hand_in, 4),
+            out_shape=[jax.ShapeDtypeStruct(a.shape, a.dtype) for a in made],
+            in_specs=[any_spec] * 4,
+            out_specs=[any_spec] * 4,
+            scratch_shapes=[pltpu.VMEM(a.shape, a.dtype) for a in made] + [dma((2, 4))],
+        )(*made)
         weights = tuple(w.reshape(1, F * rows, cols) for w in (gate_out, up_out, down_out))
-        return (*weights, mixed)
+        return (*weights, mixed.T)
 
     in_specs = (
         P(("grp", "fs"), None),

time: 190 us -> 178 us (0.937)
  local copies, waits for them, and re-layouts: 7.78 us -> 0 us
  Pallas kernels: 179 us -> 175 us
    unnamed x12 -> x0, local copies, waits for them, and re-layouts: 7.78 us -> none
    pallas_call x1, Pallas kernels: 179 us -> 173 us  [on_device(): pl.pallas_call(functools.partial(kernel, (G, F, Y, cap, nsub)), out_shape...]
    pallas_call x0 -> x1, Pallas kernels: none -> 2.25 us  [on_device(): pl.pallas_call(functools.partial(hand_in, 4), out_shape=[jax.ShapeDtypeSt...]
where the time goes in v2:
time: 178 us; the launch traced here: 176 us
  Pallas kernels  175 us (98%)
    pallas_call x1, Pallas kernels, on_device(): pl.pallas_call(functools.partial(kernel, (G, F, Y, cap, nsub)), out_shape...  173 us

profile of v2, /device:TPU:6, one launch (start us, length us, event | category | flops | bytes accessed | tf_op | source)
XLA Modules:
  0.0 175.8 jit_solution(16253218907723737884)
XLA Ops:
  0.6 172.9 %shard_map.102 = (bf16[1,16,128,128]{3,2,1,0:T(8,128)(2,1)}, bf16[1,16,128,128]{3,2,1,0:T(8,128)(2,1)}, bf16[1,16,128,128]{3,2,1,0:T(8,128)(2,1)}, bf16[64,256]{1,0:T(8,128)(2,1)}) custom-call(bf16[256,2048]{1,0:T(8,128)(2,1)} %tokens_hbm.1, s32[2,256]{1,0:T(2,128)} %bitcast.7, f32[2,256]{1,0:T(2,128)} %bitcast.8, f32[1,128]{1,0:T(1,128)} %bitcast.9, ...), custom_call_target="tpu_custom_call" | custom-call | tf_op jit(solution)/shard_map/pallas_call | solution.py:580
  173.5 2.3 %shard_map.103 = (bf16[1,16,128,128]{3,2,1,0:T(8,128)(2,1)}, bf16[1,16,128,128]{3,2,1,0:T(8,128)(2,1)}, bf16[1,16,128,128]{3,2,1,0:T(8,128)(2,1)}, bf16[64,256]{1,0:T(8,128)(2,1)}) custom-call(bf16[1,16,128,128]{3,2,1,0:T(8,128)(2,1)} %get-tuple-element.12.refs_0_, bf16[1,16,128,128]{3,2,1,0:T(8,128)(2,1)} %get-tuple-element.13.refs_1_, ...), custom_call_target="tpu_custom_call" | custom-call | tf_op jit(solution)/shard_map/pallas_call | solution.py:634

commit v3 on v2

--- a/solution.py
+++ b/solution.py
@@ -52,8 +52,11 @@
     rs_lsend,
     rs_rrecv,
     rs_lrecv,
+    near_send,
+    near_recv,
     ret_send,
     ret_recv,
+    key_tab,
     share_tab,
     mix_own,
     mix_other,
@@ -71,6 +74,8 @@
     agr_r,
     agl_s,
     agl_r,
+    near_s,
+    near_r,
     rsr_s,
     rsr_r,
     rsl_s,
@@ -80,9 +85,10 @@
     mix_s,
     mix_r,
 ):
-    G, F, Y, cap, nsub = dims
+    G, F, Y, cap, nsub, nsum = dims
     half = F // 2
     per = half // nsub
+    sum_per = half // nsum
     right_steps, left_steps = Y // 2, Y // 2 - 1
     rows = wsend.shape[2]
     share = rows // G
@@ -166,12 +172,14 @@
     pick[0] = jnp.where(key_first == ident, 1.0, 0.0).astype(BF16)
     pick[1] = jnp.where(key_second == ident, 1.0, 0.0).astype(BF16)
 
+    key_tab[0] = jnp.broadcast_to(key_first, (tok, lanes))
+    key_tab[1] = jnp.broadcast_to(key_second, (tok, lanes))
     diff = table[:, 2:3] - table[:, 3:4]
     share_tab[0] = jnp.broadcast_to(1.0 / (1.0 + jnp.exp(-diff)), (tok, lanes))
     share_tab[1] = jnp.broadcast_to(1.0 / (1.0 + jnp.exp(diff)), (tok, lanes))
 
     loads[0].wait()
-    chunk = 32
+    chunk = 64
 
     def norm(i):
         at = pl.ds(pl.multiple_of(i * chunk, chunk), chunk)
@@ -316,8 +324,14 @@
             device_id_type=MESH,
         )
 
-    for j in range(nsub):
-        for k in range(j * per, (j + 1) * per):
+    own_part = lax.div(lax.div(me, 2), per)
+    near = [lax.rem(own_part + nsub + (j + 1) // 2 * (1 - j % 2 * 2), nsub) for j in range(nsub)]
+    own_sum = lax.div(lax.div(me, 2), sum_per)
+    far = [lax.rem(own_sum + nsum - 1 - j, nsum) for j in range(nsum)]
+
+    for j in near:
+        for n in range(per):
+            k = j * per + n
 
             @pl.when(2 * k + par != me)
             def _(k=k):
@@ -327,7 +341,7 @@
         ag_copy(0, j, False).start()
 
     def ag_step(i, both):
-        for j in range(nsub):
+        for j in near:
             ag_copy(i - 1, j, True).wait_recv()
             ag_copy(i, j, True).start()
             ag_copy(i - 1, j, False).wait_recv()
@@ -359,59 +373,6 @@
         send_weights(1)
 
     loop(right_steps, F // 2 + 2, tend)
-    taken(d_r.at[0], wpart.at[kinds[0]])
-    store_g = pltpu.make_async_copy(wown.at[0], go_hbm.at[0], store_sem.at[0])
-    store_u = pltpu.make_async_copy(wown.at[1], uo_hbm.at[0], store_sem.at[1])
-    store_g.start()
-    store_u.start()
-
-    acc_g[...] = jnp.zeros_like(acc_g)
-    acc_u[...] = jnp.zeros_like(acc_u)
-    area = half * cap
-
-    def contract(a, b):
-        lhs = jnp.concatenate(
-            [xb[a].reshape(area, feats), xb[b].reshape(area, feats)], axis=1
-        )
-
-        def rhs(p):
-            top = jnp.concatenate([wown[p, a], wpart[p, a]], axis=1)
-            low = jnp.concatenate([wown[p, b], wpart[p, b]], axis=1)
-            return jnp.concatenate([top, low], axis=0)
-
-        acc_g[...] += jnp.dot(lhs, rhs(0), preferred_element_type=F32)
-        acc_u[...] += jnp.dot(lhs, rhs(1), preferred_element_type=F32)
-
-    loop(1, left_steps + 1, lambda i: contract(lax.rem(y + Y - i, Y), lax.rem(y + i, Y)))
-    for j in range(nsub):
-        ag_copy(right_steps - 1, j, True).wait_recv()
-    contract(y, lax.rem(y + right_steps, Y))
-
-    def activate(k):
-        at = pl.ds(pl.multiple_of(k * cap, cap), cap)
-        v = acc_g[at, :]
-        hid[at, :] = (v / (1.0 + jnp.exp(-v)) * acc_u[at, :]).astype(BF16)
-
-    loop(0, half, activate)
-
-    def product(d):
-        block = jnp.concatenate([wown[2, d], wpart[2, d]], axis=1)
-        return lax.dot_general(
-            hid[...], block, (((1,), (1,)), ((), ())), preferred_element_type=F32
-        )
-
-    sub = per * cap
-
-    def rs_copy(i, j, to_right):
-        return pltpu.make_async_remote_copy(
-            src_ref=(rs_rsend if to_right else rs_lsend).at[i, j],
-            dst_ref=(rs_rrecv if to_right else rs_lrecv).at[i, j],
-            send_sem=rsr_s if to_right else rsl_s,
-            recv_sem=(rsr_r if to_right else rsl_r).at[i, j],
-            device_id={"tp": right if to_right else left},
-            device_id_type=MESH,
-        )
-
     def right_chunk(i):
         return lax.rem(y + right_steps + Y - i, Y)
 
@@ -441,83 +402,82 @@
 
     for n in range(4):
         down_block(pass_on, n)
+    taken(d_r.at[0], wpart.at[kinds[0]])
+    store_g = pltpu.make_async_copy(wown.at[0], go_hbm.at[0], store_sem.at[0])
+    store_u = pltpu.make_async_copy(wown.at[1], uo_hbm.at[0], store_sem.at[1])
+    store_g.start()
+    store_u.start()
+
+    acc_g[...] = jnp.zeros_like(acc_g)
+    acc_u[...] = jnp.zeros_like(acc_u)
+    area = half * cap
+
+    def contract(a, b):
+        lhs = jnp.concatenate(
+            [xb[a].reshape(area, feats), xb[b].reshape(area, feats)], axis=1
+        )
+
+        def rhs(p):
+            top = jnp.concatenate([wown[p, a], wpart[p, a]], axis=1)
+            low = jnp.concatenate([wown[p, b], wpart[p, b]], axis=1)
+            return jnp.concatenate([top, low], axis=0)
+
+        acc_g[...] += jnp.dot(lhs, rhs(0), preferred_element_type=F32)
+        acc_u[...] += jnp.dot(lhs, rhs(1), preferred_element_type=F32)
+
+    loop(1, left_steps + 1, lambda i: contract(lax.rem(y + Y - i, Y), lax.rem(y + i, Y)))
     for n in range(2):
         down_block(hand_over, n)
+    for j in near:
+        ag_copy(right_steps - 1, j, True).wait_recv()
+    contract(y, lax.rem(y + right_steps, Y))
+
+    def activate(k):
+        at = pl.ds(pl.multiple_of(k * cap, cap), cap)
+        v = acc_g[at, :]
+        hid[at, :] = (v / (1.0 + jnp.exp(-v)) * acc_u[at, :]).astype(BF16)
+
+    loop(0, half, activate)
+
+    def product(d):
+        block = jnp.concatenate([wown[2, d], wpart[2, d]], axis=1)
+        return lax.dot_general(
+            hid[...], block, (((1,), (1,)), ((), ())), preferred_element_type=F32
+        )
+
+    sub = sum_per * cap
     down_ready(0)
-    part_r[...] = product(right_chunk(0))
-    for j in range(nsub):
-        rs_rsend[0, j] = part_r[pl.ds(j * sub, sub), :].astype(BF16)
-        rs_copy(0, j, True).start()
-    part_l[...] = product(left_chunk(0))
-    for j in range(nsub):
-        rs_lsend[0, j] = part_l[pl.ds(j * sub, sub), :].astype(BF16)
-        rs_copy(0, j, False).start()
-
-    def rs_step(i, both):
-        down_ready(i)
-        part_r[...] = product(right_chunk(i))
-        if both:
-            part_l[...] = product(left_chunk(i))
-        for j in range(nsub):
-            at = pl.ds(j * sub, sub)
-            rs_copy(i - 1, j, True).wait_recv()
-            rs_rsend[i, j] = (rs_rrecv[i - 1, j].astype(F32) + part_r[at, :]).astype(BF16)
-            rs_copy(i, j, True).start()
-            if both:
-                rs_copy(i - 1, j, False).wait_recv()
-                rs_lsend[i, j] = (rs_lrecv[i - 1, j].astype(F32) + part_l[at, :]).astype(BF16)
-                rs_copy(i, j, False).start()
-
-    loop(1, left_steps, lambda i: rs_step(i, True))
-    for i in range(max(1, left_steps), right_steps):
-        rs_step(i, False)
-
-    def ret_copy(k):
-        return pltpu.make_async_remote_copy(
-            src_ref=ret_send.at[k],
-            dst_ref=ret_recv.at[lax.div(me, 2)],
+
+    def near_copy(n):
+        return pltpu.make_async_remote_copy(
+            src_ref=near_send.at[n],
+            dst_ref=near_recv.at[n],
+            send_sem=near_s,
+            recv_sem=near_r.at[n],
+            device_id={"tp": partner},
+            device_id_type=MESH,
+        )
+
+    def rs_copy(i, h, j, to_right):
+        return pltpu.make_async_remote_copy(
+            src_ref=(rs_rsend if to_right else rs_lsend).at[i, h, j],
+            dst_ref=(rs_rrecv if to_right else rs_lrecv).at[i, h, j],
+            send_sem=rsr_s if to_right else rsl_s,
+            recv_sem=(rsr_r if to_right else rsl_r).at[i, h, j],
+            device_id={"tp": right if to_right else left},
+            device_id_type=MESH,
+        )
+
+    def ret_copy(h, k):
+        return pltpu.make_async_remote_copy(
+            src_ref=ret_send.at[h, k],
+            dst_ref=ret_recv.at[me],
             send_sem=ret_s,
             recv_sem=ret_r,
-            device_id={"fs": 2 * k + par},
-            device_id_type=MESH,
-        )
-
-    store_d = pltpu.make_async_copy(wown.at[2], do_hbm.at[0], store_sem.at[2])
-    store_d.start()
-    part_r[...] = product(y)
-    for j in range(nsub):
-        rs_copy(left_steps - 1, j, False).wait_recv()
-        rs_copy(right_steps - 1, j, True).wait_recv()
-        total = (
-            part_r[pl.ds(j * sub, sub), :]
-            + rs_rrecv[right_steps - 1, j].astype(F32)
-            + rs_lrecv[left_steps - 1, j].astype(F32)
-        ).astype(BF16)
-        ret_send[pl.ds(j * per, per)] = total.reshape(per, cap, feats)
-        for k in range(j * per, (j + 1) * per):
-
-            @pl.when(2 * k + par != me)
-            def _(k=k):
-                ret_copy(k).start()
-
-    @pl.when(c == 0)
-    def _():
-        ret_recv[lax.div(me, 2)] = ret_send[lax.div(me, 2)]
-
-    def all_but_own(sem, ref):
-        @pl.when(c == 0)
-        def _():
-            taken(sem, ref.at[pl.ds(0, half - 1)])
-
-        @pl.when(c == 1)
-        def _():
-            taken(sem, ref)
-
-    all_but_own(ret_r, ret_recv)
-    returned = ret_recv[...].reshape(area, feats)
-    mix_own[...] = share_tab[0] * jnp.dot(
-        pick[0], returned, preferred_element_type=F32
-    ) + share_tab[1] * jnp.dot(pick[1], returned, preferred_element_type=F32)
+            device_id={"fs": 2 * k + lax.rem(me + h, 2)},
+            device_id_type=MESH,
+        )
+
     swap = pltpu.make_async_remote_copy(
         src_ref=mix_own,
         dst_ref=mix_other,
@@ -526,26 +486,134 @@
         device_id={"tp": partner},
         device_id_type=MESH,
     )
-    swap.start()
-    swap.wait_recv()
-    both = (mix_own[...] + mix_other[...]).T
-    width = mix_ref.shape[0]
-    mix_ref[...] = jnp.where(c == 0, both[:width, :], both[width:, :]).astype(BF16)
-
-    swap.wait_send()
+
+    @pl.when(c == 0)
+    def _():
+        def give(n):
+            near_send[n] = product(chunk_of(n)).astype(BF16)
+            near_copy(n).start()
+
+        give(0)
+        give(1)
+
+        def give_two(i):
+            down_ready(i)
+            give(2 * i)
+            give(2 * i + 1)
+
+        loop(1, right_steps, give_two)
+
+    @pl.when(c == 1)
+    def _():
+        def rows_of(j):
+            return pl.ds(pl.multiple_of(j * sub, sub), sub)
+
+        def terms(i, both):
+            part_r[...] = product(right_chunk(i))
+            if both:
+                part_l[...] = product(left_chunk(i))
+
+        def others(i):
+            near_copy(2 * i).wait_recv()
+            near_copy(2 * i + 1).wait_recv()
+
+        def term(h, n, part, j):
+            return part[rows_of(j), :] if h else near_recv[n, rows_of(j), :].astype(F32)
+
+        terms(0, True)
+        for h in (1, 0):
+            if h == 0:
+                others(0)
+            for j in far:
+                rs_rsend[0, h, j] = term(h, 0, part_r, j).astype(BF16)
+                rs_copy(0, h, j, True).start()
+                rs_lsend[0, h, j] = term(h, 1, part_l, j).astype(BF16)
+                rs_copy(0, h, j, False).start()
+
+        def rs_step(i, both):
+            down_ready(i)
+            terms(i, both)
+            for h in (1, 0):
+                if h == 0:
+                    others(i)
+                for j in far:
+                    rs_copy(i - 1, h, j, True).wait_recv()
+                    rs_rsend[i, h, j] = (
+                        rs_rrecv[i - 1, h, j].astype(F32) + term(h, 2 * i, part_r, j)
+                    ).astype(BF16)
+                    rs_copy(i, h, j, True).start()
+                    if both:
+                        rs_copy(i - 1, h, j, False).wait_recv()
+                        rs_lsend[i, h, j] = (
+                            rs_lrecv[i - 1, h, j].astype(F32) + term(h, 2 * i + 1, part_l, j)
+                        ).astype(BF16)
+                        rs_copy(i, h, j, False).start()
+
+        loop(1, left_steps, lambda i: rs_step(i, True))
+        for i in range(max(1, left_steps), right_steps):
+            rs_step(i, False)
+
+        part_r[...] = product(y)
+        for h in (1, 0):
+            for j in far:
+                rs_copy(left_steps - 1, h, j, False).wait_recv()
+                rs_copy(right_steps - 1, h, j, True).wait_recv()
+                total = (
+                    term(h, F - 1, part_r, j)
+                    + rs_rrecv[right_steps - 1, h, j].astype(F32)
+                    + rs_lrecv[left_steps - 1, h, j].astype(F32)
+                ).astype(BF16)
+                ret_send[h, pl.ds(j * sum_per, sum_per)] = total.reshape(sum_per, cap, feats)
+                for n in range(sum_per):
+                    k = j * sum_per + n
+
+                    @pl.when(2 * k + lax.rem(me + h, 2) != me)
+                    def _(h=h, k=k):
+                        ret_copy(h, k).start()
+
+        ret_recv[me] = ret_send[0, lax.div(me, 2)]
+        slots = lax.broadcasted_iota(jnp.int32, (1, F * cap), 1).astype(F32)
+        chosen = [jnp.where(key_tab[n, :, 0:1] == slots, 1.0, 0.0).astype(BF16) for n in (0, 1)]
+        taken(ret_r, ret_recv.at[pl.ds(0, F - 1)])
+        returned = ret_recv[...].reshape(F * cap, feats)
+        both = (
+            share_tab[0] * jnp.dot(chosen[0], returned, preferred_element_type=F32)
+            + share_tab[1] * jnp.dot(chosen[1], returned, preferred_element_type=F32)
+        ).T.astype(BF16)
+        width = mix_ref.shape[0]
+        mix_own[...] = both[:width, :]
+        swap.start()
+        mix_ref[...] = both[width:, :]
+
+    store_d = pltpu.make_async_copy(wown.at[2], do_hbm.at[0], store_sem.at[2])
+    store_d.start()
+
+    @pl.when(c == 0)
+    def _():
+        swap.wait_recv()
+        mix_ref[...] = mix_other[...]
+
     for copy in (store_g, store_u, store_d):
         copy.wait()
-
-    all_but_own(tok_s, dsend)
-    all_but_own(ret_s, ret_send)
     taken(z_s, wsend.at[pl.ds(0, F - 1), :, mine])
     for n in range(1, G):
         taken(x_s.at[n - 1], wown.at[:, pl.ds(0, F - 1), mine])
     taken(d_s, wown)
     taken(agr_s, xb.at[pl.ds(0, right_steps)])
     taken(agl_s, xb.at[pl.ds(0, left_steps)])
-    taken(rsr_s, rs_rsend)
-    taken(rsl_s, rs_lsend)
+
+    @pl.when(c == 0)
+    def _():
+        taken(tok_s, dsend.at[pl.ds(0, half - 1)])
+        taken(near_s, near_send)
+
+    @pl.when(c == 1)
+    def _():
+        taken(tok_s, dsend)
+        swap.wait_send()
+        taken(ret_s, ret_recv.at[pl.ds(0, F - 1)])
+        taken(rsr_s, rs_rsend)
+        taken(rsl_s, rs_lsend)
 
 
 def hand_in(n, *refs):
@@ -569,7 +637,7 @@
         tok, width = tokens.shape
         cap = 3 * tok // experts
         half = F // 2
-        nsub = min(4, half)
+        nsub, nsum = min(4, half), min(2, half)
         feats = width // Y
         area = half * cap
         rs, ls = Y // 2, Y // 2 - 1
@@ -578,7 +646,7 @@
         dma = pltpu.SemaphoreType.DMA
         out = jax.ShapeDtypeStruct((1, F, rows, cols), BF16)
         made = pl.pallas_call(
-            functools.partial(kernel, (G, F, Y, cap, nsub)),
+            functools.partial(kernel, (G, F, Y, cap, nsub, nsum)),
             out_shape=(out, out, out, jax.ShapeDtypeStruct((feats // 2, tok), BF16)),
             in_specs=[any_spec, vmem, vmem, vmem, any_spec, any_spec, any_spec],
             out_specs=(any_spec, any_spec, any_spec, vmem),
@@ -597,15 +665,18 @@
                 pltpu.VMEM((area, 2 * cols), F32),
                 pltpu.VMEM((area, feats), F32),
                 pltpu.VMEM((area, feats), F32),
-                pltpu.VMEM((rs, nsub, area // nsub, feats), BF16),
-                pltpu.VMEM((ls, nsub, area // nsub, feats), BF16),
-                pltpu.VMEM((rs, nsub, area // nsub, feats), BF16),
-                pltpu.VMEM((ls, nsub, area // nsub, feats), BF16),
-                pltpu.VMEM((half, cap, feats), BF16),
-                pltpu.VMEM((half, cap, feats), BF16),
+                pltpu.VMEM((rs, 2, nsum, area // nsum, feats), BF16),
+                pltpu.VMEM((ls, 2, nsum, area // nsum, feats), BF16),
+                pltpu.VMEM((rs, 2, nsum, area // nsum, feats), BF16),
+                pltpu.VMEM((ls, 2, nsum, area // nsum, feats), BF16),
+                pltpu.VMEM((F, area, feats), BF16),
+                pltpu.VMEM((F, area, feats), BF16),
+                pltpu.VMEM((2, half, cap, feats), BF16),
+                pltpu.VMEM((F, cap, feats), BF16),
                 pltpu.VMEM((2, tok, feats), F32),
-                pltpu.VMEM((tok, feats), F32),
-                pltpu.VMEM((tok, feats), F32),
+                pltpu.VMEM((2, tok, feats), F32),
+                pltpu.VMEM((feats // 2, tok), BF16),
+                pltpu.VMEM((feats // 2, tok), BF16),
                 dma((4,)),
                 dma((3,)),
                 dma,
@@ -621,9 +692,11 @@
                 dma,
                 dma((ls, nsub)),
                 dma,
-                dma((rs, nsub)),
-                dma,
-                dma((ls, nsub)),
+                dma((F,)),
+                dma,
+                dma((rs, 2, nsum)),
+                dma,
+                dma((ls, 2, nsum)),
                 dma,
                 dma,
                 dma,

time: 178 us -> 175 us (0.983)
  Pallas kernels: 175 us -> 172 us
    pallas_call x1, Pallas kernels: 173 us -> 169 us  [on_device(): pl.pallas_call(functools.partial(kernel, (G, F, Y, cap, nsub, nsum)), out...]
where the time goes in v3:
time: 175 us; the launch traced here: 172 us
  Pallas kernels  172 us (98%)
    pallas_call x1, Pallas kernels, on_device(): pl.pallas_call(functools.partial(kernel, (G, F, Y, cap, nsub, nsum)), out...  169 us

profile of v3, /device:TPU:6, one launch (start us, length us, event | category | flops | bytes accessed | tf_op | source)
XLA Modules:
  0.0 172.3 jit_solution(2045039648155292165)
XLA Ops:
  0.6 169.4 %shard_map.102 = (bf16[1,16,128,128]{3,2,1,0:T(8,128)(2,1)}, bf16[1,16,128,128]{3,2,1,0:T(8,128)(2,1)}, bf16[1,16,128,128]{3,2,1,0:T(8,128)(2,1)}, bf16[64,256]{1,0:T(8,128)(2,1)}) custom-call(bf16[256,2048]{1,0:T(8,128)(2,1)} %tokens_hbm.1, s32[2,256]{1,0:T(2,128)} %bitcast.7, f32[2,256]{1,0:T(2,128)} %bitcast.8, f32[1,128]{1,0:T(1,128)} %bitcast.9, ...), custom_call_target="tpu_custom_call" | custom-call | tf_op jit(solution)/shard_map/pallas_call | solution.py:648
  170.1 2.3 %shard_map.103 = (bf16[1,16,128,128]{3,2,1,0:T(8,128)(2,1)}, bf16[1,16,128,128]{3,2,1,0:T(8,128)(2,1)}, bf16[1,16,128,128]{3,2,1,0:T(8,128)(2,1)}, bf16[64,256]{1,0:T(8,128)(2,1)}) custom-call(bf16[1,16,128,128]{3,2,1,0:T(8,128)(2,1)} %get-tuple-element.12.refs_0_, bf16[1,16,128,128]{3,2,1,0:T(8,128)(2,1)} %get-tuple-element.13.refs_1_, ...), custom_call_target="tpu_custom_call" | custom-call | tf_op jit(solution)/shard_map/pallas_call | solution.py:707

commit v4 on v3

--- a/solution.py
+++ b/solution.py
@@ -267,7 +267,7 @@
             src_ref=wown.at[kinds[kind], s],
             dst_ref=wpart.at[kinds[kind], s],
             send_sem=d_s,
-            recv_sem=d_r.at[kind * (s + 1)],
+            recv_sem=d_r.at[kind, s],
             device_id={"tp": partner},
             device_id_type=MESH,
         )
@@ -372,7 +372,37 @@
     def _():
         send_weights(1)
 
-    loop(right_steps, F // 2 + 2, tend)
+    tend(right_steps)
+
+    acc_g[...] = jnp.zeros_like(acc_g)
+    acc_u[...] = jnp.zeros_like(acc_u)
+    area = half * cap
+
+    def contract(a, b):
+        lhs = jnp.concatenate(
+            [xb[a].reshape(area, feats), xb[b].reshape(area, feats)], axis=1
+        )
+
+        def rhs(p):
+            top = jnp.concatenate([wown[p, a], wpart[p, a]], axis=1)
+            low = jnp.concatenate([wown[p, b], wpart[p, b]], axis=1)
+            return jnp.concatenate([top, low], axis=0)
+
+        acc_g[...] += jnp.dot(lhs, rhs(0), preferred_element_type=F32)
+        acc_u[...] += jnp.dot(lhs, rhs(1), preferred_element_type=F32)
+
+    def contract_pair(i):
+        a, b = lax.rem(me + i, F), lax.rem(me + F - i, F)
+        d_copy(0, a).wait_recv()
+        d_copy(0, b).wait_recv()
+        contract(a, b)
+
+    for j in near:
+        ag_copy(right_steps - 1, j, True).wait_recv()
+    pairs = max(1, left_steps - 1)
+    loop(1, pairs, contract_pair)
+    loop(right_steps + 1, F // 2 + 2, tend)
+
     def right_chunk(i):
         return lax.rem(y + right_steps + Y - i, Y)
 
@@ -402,35 +432,18 @@
 
     for n in range(4):
         down_block(pass_on, n)
-    taken(d_r.at[0], wpart.at[kinds[0]])
     store_g = pltpu.make_async_copy(wown.at[0], go_hbm.at[0], store_sem.at[0])
     store_u = pltpu.make_async_copy(wown.at[1], uo_hbm.at[0], store_sem.at[1])
     store_g.start()
     store_u.start()
 
-    acc_g[...] = jnp.zeros_like(acc_g)
-    acc_u[...] = jnp.zeros_like(acc_u)
-    area = half * cap
-
-    def contract(a, b):
-        lhs = jnp.concatenate(
-            [xb[a].reshape(area, feats), xb[b].reshape(area, feats)], axis=1
-        )
-
-        def rhs(p):
-            top = jnp.concatenate([wown[p, a], wpart[p, a]], axis=1)
-            low = jnp.concatenate([wown[p, b], wpart[p, b]], axis=1)
-            return jnp.concatenate([top, low], axis=0)
-
-        acc_g[...] += jnp.dot(lhs, rhs(0), preferred_element_type=F32)
-        acc_u[...] += jnp.dot(lhs, rhs(1), preferred_element_type=F32)
-
-    loop(1, left_steps + 1, lambda i: contract(lax.rem(y + Y - i, Y), lax.rem(y + i, Y)))
+    loop(pairs, left_steps + 1, contract_pair)
     for n in range(2):
         down_block(hand_over, n)
-    for j in near:
-        ag_copy(right_steps - 1, j, True).wait_recv()
-    contract(y, lax.rem(y + right_steps, Y))
+    opposite = lax.rem(me + right_steps, F)
+    d_copy(0, me).wait_recv()
+    d_copy(0, opposite).wait_recv()
+    contract(me, opposite)
 
     def activate(k):
         at = pl.ds(pl.multiple_of(k * cap, cap), cap)
@@ -686,7 +699,7 @@
                 dma((max(G - 1, 1),)),
                 dma((2, max(G - 1, 1), F)),
                 dma,
-                dma((F + 1,)),
+                dma((2, F)),
                 dma,
                 dma((rs, nsub)),
                 dma,

time: 175 us -> 176 us (level)
  no operation moved by 1% of the time
where the time goes in v4:
time: 176 us; the launch traced here: 173 us
  Pallas kernels  172 us (98%)
    pallas_call x1, Pallas kernels, on_device(): pl.pallas_call(functools.partial(kernel, (G, F, Y, cap, nsub, nsum)), out...  170 us

profile of v4, /device:TPU:6, one launch (start us, length us, event | category | flops | bytes accessed | tf_op | source)
XLA Modules:
  0.0 172.9 jit_solution(2824750202920025)
XLA Ops:
  0.6 170.0 %shard_map.102 = (bf16[1,16,128,128]{3,2,1,0:T(8,128)(2,1)}, bf16[1,16,128,128]{3,2,1,0:T(8,128)(2,1)}, bf16[1,16,128,128]{3,2,1,0:T(8,128)(2,1)}, bf16[64,256]{1,0:T(8,128)(2,1)}) custom-call(bf16[256,2048]{1,0:T(8,128)(2,1)} %tokens_hbm.1, s32[2,256]{1,0:T(2,128)} %bitcast.7, f32[2,256]{1,0:T(2,128)} %bitcast.8, f32[1,128]{1,0:T(1,128)} %bitcast.9, ...), custom_call_target="tpu_custom_call" | custom-call | tf_op jit(solution)/shard_map/pallas_call | solution.py:661
  170.6 2.3 %shard_map.103 = (bf16[1,16,128,128]{3,2,1,0:T(8,128)(2,1)}, bf16[1,16,128,128]{3,2,1,0:T(8,128)(2,1)}, bf16[1,16,128,128]{3,2,1,0:T(8,128)(2,1)}, bf16[64,256]{1,0:T(8,128)(2,1)}) custom-call(bf16[1,16,128,128]{3,2,1,0:T(8,128)(2,1)} %get-tuple-element.12.refs_0_, bf16[1,16,128,128]{3,2,1,0:T(8,128)(2,1)} %get-tuple-element.13.refs_1_, ...), custom_call_target="tpu_custom_call" | custom-call | tf_op jit(solution)/shard_map/pallas_call | solution.py:720
